TPU v7x, 32 devices: a whole 2x2x4 slice. The times are simulated.
32 devices in a mesh: sp: 8 (over z, y), tp: 4 (over x, core).
Axes of the slice: x: 2, y: 2, z: 4, core: 2. Of those that a mesh axis runs over, the one named last changes fastest.
Arguments:
- out_grad: bfloat16 [1024, 2048], P('sp', 'tp'), may hold values from -6 to 6
- route_ids: int32 [1024, 2], P('sp'), may hold values from 0 to 7, as said below
- route_weight: float32 [1024, 2], P('sp'), may hold values from 0.1 to 0.9
- expert_inputs: bfloat16 [8, 512, 2048], P('sp'), may hold values from -6 to 6
- gate_weight: bfloat16 [8, 2048, 3072], P('sp', None, 'tp'), may hold values from -0.125 to 0.125
- up_weight: bfloat16 [8, 2048, 3072], P('sp', None, 'tp'), may hold values from -0.125 to 0.125
- down_weight: bfloat16 [8, 3072, 2048], P('sp', 'tp'), may hold values from -0.109375 to 0.109375
- out_gate: bfloat16 [1024, 2048], P('sp', 'tp'), may hold values from -6 to 6
- in_gate: bfloat16 [1024, 2048], P('sp', 'tp'), may hold values from -6 to 6
- values: bfloat16 [1024, 2048], P('sp', 'tp'), may hold values from -6 to 6
- conv_out: bfloat16 [1024, 2048], P('sp', 'tp'), may hold values from -6 to 6
- conv_taps: bfloat16 [3, 2048], P(None, 'tp'), may hold values from -3.5 to 3.5
- proj_weight: bfloat16 [2048, 2048], P(None, 'tp'), may hold values from -0.125 to 0.125
Outputs:
- resid_grad: bfloat16 [1024, 2048], P('sp', 'tp')
- out_gate_grad: bfloat16 [1024, 2048], P('sp', 'tp')
- in_gate_grad: bfloat16 [1024, 2048], P('sp', 'tp')
- values_grad: bfloat16 [1024, 2048], P('sp', 'tp')
- proj_grad: float32 [2048, 2048], P('sp', 'tp')
- gate_grad: bfloat16 [8, 2048, 3072], P('sp', None, 'tp')
- up_grad: bfloat16 [8, 2048, 3072], P('sp', None, 'tp')
- down_grad: bfloat16 [8, 3072, 2048], P('sp', 'tp')
Inputs may be any that keep to these rules, and one draw needn't show every extreme that they name: `route_ids`: each row names two different experts. Among the rows of one device (aligned blocks of 128 rows) no expert is named more than 64 times, and in every draw one expert is named exactly 64 times in every block.
All inputs are finite; a program needn't handle non-finite values.
Results may differ from a plain program's by a relative error of at most 0.017.
Values may be sent and summed in bfloat16 or wider, within the bound.
A program may use at most 128 MiB of HBM per device.

v0:
```python
import math
import jax
import jax.numpy as jnp
from jax import lax
from jax.sharding import PartitionSpec as P


def extended(x, sides, width):
    for axis, dim in sides:
        devices, length = (lax.axis_size(axis), x.shape[dim])
        up = [(i, (i + 1) % devices) for i in range(devices - 1)]
        down = [(j, i) for i, j in up]
        last = lax.slice_in_dim(x, length - width, length, axis=dim)
        first = lax.slice_in_dim(x, 0, width, axis=dim)
        before = lax.ppermute(last, axis, up)
        after = lax.ppermute(first, axis, down)
        x = jnp.concatenate([before, x, after], axis=dim)
    return x


def contract_first(left, right):
    return lax.dot_general(
        left, right, (((0,), (0,)), ((), ())), preferred_element_type=jnp.float32
    )


def contract_last(left, right):
    return lax.dot_general(
        left, right, (((1,), (1,)), ((), ())), preferred_element_type=jnp.float32
    )


def expert_backward(inputs, routed, gate_w, up_w, down_w):
    pre_gate = jnp.dot(inputs, gate_w, preferred_element_type=jnp.float32)
    pre_up = jnp.dot(inputs, up_w, preferred_element_type=jnp.float32)
    sigmoid_g = jax.nn.sigmoid(pre_gate)
    activated = pre_gate * sigmoid_g
    hidden = (activated * pre_up).astype(jnp.bfloat16)
    d_hidden = contract_last(routed, down_w)
    d_gate = (d_hidden * pre_up * sigmoid_g * (1.0 + pre_gate * (1.0 - sigmoid_g))).astype(
        jnp.bfloat16
    )
    d_up = (d_hidden * activated).astype(jnp.bfloat16)
    partial_value = contract_last(d_gate, gate_w) + contract_last(d_up, up_w)
    grad_set = (
        contract_first(inputs, d_gate),
        contract_first(inputs, d_up),
        contract_first(hidden, routed),
    )
    return (partial_value, grad_set)


def expert_pass(outgoing, input_rows, gate_weight, up_weight, down_weight):
    arrived = lax.all_to_all(outgoing, "sp", split_axis=0, concat_axis=1, tiled=True)
    routed = lax.all_gather(arrived, "tp", axis=2, tiled=True)
    partial_value, grad_set = expert_backward(
        input_rows[0], routed[0], gate_weight[0], up_weight[0], down_weight[0]
    )
    partials = [partial_value]
    gate_list = [grad_set[0]]
    up_list = [grad_set[1]]
    down_list = [grad_set[2]]
    summed = lax.psum_scatter(
        jnp.stack(partials).astype(jnp.bfloat16), "tp", scatter_dimension=2, tiled=True
    )
    returned = lax.all_to_all(summed, "sp", split_axis=1, concat_axis=0, tiled=True)
    return (returned, (jnp.stack(gate_list), jnp.stack(up_list), jnp.stack(down_list)))


def per_device(
    out_grad,
    route_ids,
    route_weight,
    expert_inputs,
    gate_weight,
    up_weight,
    down_weight,
    out_gate,
    in_gate,
    values,
    conv_out,
    conv_taps,
    proj_weight,
):
    sp_devices = lax.axis_size("sp")
    tok_rows = out_grad.shape[0]
    local_experts = gate_weight.shape[0]
    all_experts = sp_devices * local_experts
    capacity = 4 * tok_rows // all_experts
    flat_ids = route_ids.reshape(-1)
    onehot = (flat_ids[:, None] == jnp.arange(all_experts, dtype=jnp.int32)[None, :]).astype(
        jnp.int32
    )
    ranked = jnp.sum((jnp.cumsum(onehot, axis=0) - onehot) * onehot, axis=1)
    slot_ids = flat_ids * capacity + ranked
    dispatch = (
        jnp.arange(all_experts * capacity, dtype=jnp.int32)[:, None] == slot_ids[None, :]
    ).astype(jnp.bfloat16)
    weighted = (
        (route_weight[:, :, None] * out_grad.astype(jnp.float32)[:, None, :])
        .astype(jnp.bfloat16)
        .reshape(2 * tok_rows, -1)
    )
    outgoing = jnp.dot(dispatch, weighted, preferred_element_type=jnp.float32).astype(jnp.bfloat16)
    outgoing = outgoing.reshape(all_experts, capacity, -1)
    returned, totals = expert_pass(outgoing, expert_inputs, gate_weight, up_weight, down_weight)
    slot_scale = 1.0 / math.sqrt(expert_inputs.shape[1])
    gate_grad = (totals[0] * slot_scale).astype(jnp.bfloat16)
    up_grad = (totals[1] * slot_scale).astype(jnp.bfloat16)
    down_grad = (totals[2] * slot_scale).astype(jnp.bfloat16)
    combiner = jnp.sum(dispatch.reshape(all_experts * capacity, tok_rows, 2), axis=2)
    moe_part = contract_first(combiner, returned.reshape(all_experts * capacity, -1))
    resid_grad = (out_grad.astype(jnp.float32) + moe_part).astype(jnp.bfloat16)
    resid_full = lax.all_gather(resid_grad, "tp", axis=1, tiled=True)
    mix_grad = jnp.dot(resid_full, proj_weight, preferred_element_type=jnp.float32)
    gate_vals = out_gate.astype(jnp.float32)
    conv_vals = conv_out.astype(jnp.float32)
    mixed_in = (gate_vals * conv_vals).astype(jnp.bfloat16)
    out_gate_grad = (mix_grad * conv_vals).astype(jnp.bfloat16)
    conv_grad = (mix_grad * gate_vals).astype(jnp.bfloat16)
    padded = extended(conv_grad, (("sp", 0),), 1).astype(jnp.float32)
    tap_vals = conv_taps.astype(jnp.float32)
    value_grad = padded[2:] * tap_vals[0] + padded[1:-1] * tap_vals[1] + padded[:-2] * tap_vals[2]
    in_gate_grad = (value_grad * values.astype(jnp.float32)).astype(jnp.bfloat16)
    values_grad = (value_grad * in_gate.astype(jnp.float32)).astype(jnp.bfloat16)
    token_scale = 1.0 / math.sqrt(tok_rows * sp_devices)
    columns = lax.all_to_all(resid_full, "sp", split_axis=1, concat_axis=0, tiled=True)
    proj_sum = contract_first(columns, lax.all_gather(mixed_in, "sp", axis=0, tiled=True))
    proj_grad = proj_sum * token_scale
    return (
        resid_grad,
        out_gate_grad,
        in_gate_grad,
        values_grad,
        proj_grad,
        gate_grad,
        up_grad,
        down_grad,
    )


def solution(mesh):
    in_specs = (
        P("sp", "tp"),
        P("sp", None),
        P("sp", None),
        P("sp", None, None),
        P("sp", None, "tp"),
        P("sp", None, "tp"),
        P("sp", "tp", None),
        P("sp", "tp"),
        P("sp", "tp"),
        P("sp", "tp"),
        P("sp", "tp"),
        P(None, "tp"),
        P(None, "tp"),
    )
    out_specs = (
        P("sp", "tp"),
        P("sp", "tp"),
        P("sp", "tp"),
        P("sp", "tp"),
        P("sp", "tp"),
        P("sp", None, "tp"),
        P("sp", None, "tp"),
        P("sp", "tp", None),
    )
    return jax.shard_map(
        per_device, mesh=mesh, in_specs=in_specs, out_specs=out_specs, check_vma=False
    )
```

profile of v0, /device:TPU:0, one launch (start us, length us, event | category | flops | bytes accessed | tf_op | source)
XLA Modules:
  0.0 198.5 jit_solution(15342331069827276)
XLA Ops:
  7.2 0.0 copy-start
  7.2 0.0 all-gather.3.cloned.1.call-start
  7.2 0.9 copy.60
  8.2 0.1 eq.50
  8.3 0.1 eq.46
  8.5 0.6 reduce-window.6
  9.0 0.2 slice_reduce_fusion
  9.3 0.1 fusion.39
  9.4 1.8 mul.130
  11.2 2.2 %mul.131 = f32[256,512]{1,0:T(8,128)} reshape(f32[128,2,512]{2,1,0:T(2,128)} %mul.130) | data formatting | bytes 1048576 | tf_op jit(solution)/shard_map/mul | solution.py:100
  13.4 0.8 copy.63
  14.2 0.1 mul.128
  14.4 1.4 convolution_convert_fusion
  15.8 21.7 %all_to_all.40 = bf16[8,64,512]{2,1,0:T(8,128)(2,1)} all-to-all(bf16[8,64,512]{2,1,0:T(8,128)(2,1)S(1)} %bitcast.88), channel_id=1, replica_groups=mesh['sp'=8,'tp'=4] {'sp'}, dimensions={0} | all-to-all | bytes 1048576 | tf_op jit(solution)/shard_map/all_to_all | solution.py:54
  37.5 0.0 all-gather.3.cloned.1.call-update
  37.6 0.0 reduce-scatter.2.cloned.1.call-start
  37.6 0.0 copy-start.9
  37.6 0.0 copy-start.11
  37.6 4.7 %fusion.2 = f32[512,768]{1,0:T(8,128)} fusion(bf16[1,2048,768]{2,1,0:T(8,128)(2,1)S(1)} %copy-done, bf16[1,512,2048]{2,1,0:T(8,128)(2,1)} %param.16), kind=kOutput, calls=%fused_computation.6 | convolution fusion | flops 1610612736 | bytes 6815744 | tf_op jit(solution)/shard_map/dot_general | solution.py:34
  42.3 3.0 %fusion.6 = f32[512,768]{1,0:T(8,128)} fusion(bf16[1,2048,768]{2,1,0:T(8,128)(2,1)S(1)} %copy-done.9, bf16[1,512,2048]{2,1,0:T(8,128)(2,1)S(1)} %copy-done.11), kind=kOutput, calls=%fused_computation.10 | convolution fusion | flops 1610612736 | bytes 6815744 | tf_op jit(solution)/shard_map/dot_general | solution.py:35
  45.3 14.0 %all-gather.3.cloned.1.call-done = bf16[1,512,2048]{2,1,0:T(8,128)(2,1)} async-done(((bf16[1,512,512]{2,1,0:T(8,128)(2,1)}), bf16[1,512,2048]{2,1,0:T(8,128)(2,1)}) %all-gather.3.cloned.1.call-update) | async-done | bytes 2097168 | tf_op jit(solution)/shard_map/all_gather | solution.py:55
  59.3 5.6 %multiply_convert_fusion.4 = (bf16[512,768]{1,0:T(8,128)(2,1)S(1)}, bf16[512,768]{1,0:T(8,128)(2,1)S(1)}) fusion(f32[512,768]{1,0:T(8,128)} %fusion.2, f32[512,768]{1,0:T(8,128)} %fusion.6, bf16[1,768,2048]{2,1,0:T(8,128)(2,1)} %param.19, bf16[1,512,2048]{2,1,0:T(8,128)(2,1)} %all-gather.3.cloned.1.call-done), kind=kOutput, calls=%fused_computation.25 | convolution fusion | flops 1615724544 | bytes 9961472 | tf_op jit(solution)/shard_map/dot_general | solution.py:28
  64.9 0.0 copy-start.10
  65.0 1.8 fusion
  66.8 0.6 copy-done.10
  67.4 3.1 %fusion.15 = bf16[1,512,2048]{2,1,0:T(8,128)(2,1)} fusion(f32[512,2048]{1,0:T(8,128)S(1)} %fusion, bf16[512,768]{1,0:T(8,128)(2,1)S(1)} %get-tuple-element.58, bf16[1,2048,768]{2,1,0:T(8,128)(2,1)S(1)} %copy-done.10), kind=kOutput, calls=%fused_computation.17 | convolution fusion | flops 1612709888 | bytes 10223616 | tf_op jit(solution)/shard_map/dot_general | solution.py:28
  70.5 0.0 reduce-scatter.2.cloned.1.call-update
  70.6 0.1 reduce_sum.24
  70.7 0.1 copy.62
  70.8 31.1 %reduce-scatter.2.cloned.1.call-done = bf16[1,512,512]{2,1,0:T(8,128)(2,1)} async-done(((bf16[1,512,2048]{2,1,0:T(8,128)(2,1)}), bf16[1,512,512]{2,1,0:T(8,128)(2,1)}) %reduce-scatter.2.cloned.1.call-update) | async-done | bytes 524304 | tf_op jit(solution)/shard_map/reduce_scatter | solution.py:63
  101.9 2.8 %copy.77 = bf16[1,512,512]{2,0,1:T(2,128)(2,1)} copy(bf16[1,512,512]{2,1,0:T(8,128)(2,1)} %reduce-scatter.2.cloned.1.call-done) | data formatting | bytes 1048576 | tf_op jit(solution)/shard_map/reduce_scatter | solution.py:63
  104.7 0.5 broadcast.62
  105.2 5.6 %reduce.3 = bf16[512,512]{1,0:T(8,128)(2,1)} reduce(bf16[512,1,512]{2,1,0:T(2,128)(2,1)} %bitcast.84, bf16[]{:T(256)} %broadcast.62), dimensions={1}, to_apply=%bitcast.82.reduce_sub_computation | reduce | bytes 1048578
  110.8 2.2 %reshape.85 = bf16[8,2,16384]{2,1,0:T(2,128)(2,1)} reshape(bf16[512,512]{1,0:T(8,128)(2,1)} %reduce.3) | data formatting | bytes 1048576
  113.0 5.5 %all-to-all-start.1 = ((bf16[8,2,16384]{2,1,0:T(2,128)(2,1)}), bf16[8,2,16384]{2,1,0:T(2,128)(2,1)}, u32[]{:S(2)}, u32[]{:S(2)}) async-start(bf16[8,2,16384]{2,1,0:T(2,128)(2,1)} %reshape.85), calls=%async_computation.2 | async-start | bytes 1048576 | tf_op jit(solution)/shard_map/all_to_all | solution.py:66
  118.5 0.2 all-gather.5.cloned.1.call-start
  118.8 0.1 fusion.33
  118.8 0.0 copy-start.3
  118.9 5.4 %fusion.10 = bf16[1,2048,768]{1,2,0:T(8,128)(2,1)} fusion(bf16[512,768]{1,0:T(8,128)(2,1)} %copy-done.13, bf16[1,512,2048]{2,1,0:T(8,128)(2,1)} %param.16), kind=kOutput, calls=%fused_computation.14 | convolution fusion | flops 1613758464 | bytes 6029312 | tf_op jit(solution)/shard_map/dot_general | solution.py:22
  124.2 8.7 %all-to-all-done.1 = bf16[8,2,16384]{2,1,0:T(2,128)(2,1)} async-done(((bf16[8,2,16384]{2,1,0:T(2,128)(2,1)}), bf16[8,2,16384]{2,1,0:T(2,128)(2,1)}, u32[]{:S(2)}, u32[]{:S(2)}) %all-to-all-start.1) | async-done | bytes 524320 | tf_op jit(solution)/shard_map/all_to_all | solution.py:66
  132.9 3.5 %reshape.86 = bf16[512,1,512]{2,1,0:T(2,128)(2,1)} reshape(bf16[8,2,16384]{2,1,0:T(2,128)(2,1)} %all-to-all-done.1) | data formatting | bytes 1048576
  136.4 1.5 fusion.25
  137.9 0.0 copy-start.4
  137.9 6.5 %all_gather.10 = bf16[128,2048]{1,0:T(8,128)(2,1)S(1)} all-gather(bf16[128,512]{1,0:T(8,128)(2,1)S(1)} %fusion.25), channel_id=1, replica_groups=mesh['sp'=8,'tp'=4] {'tp'}, dimensions={1}, use_global_device_ids=true | all-gather | bytes 655360 | tf_op jit(solution)/shard_map/all_gather | solution.py:114
  144.4 0.8 copy-done.1
  145.2 2.8 %fusion.31 = (bf16[128,512]{1,0:T(8,128)(2,1)S(1)}, bf16[128,512]{1,0:T(8,128)(2,1)}, bf16[128,512]{1,0:T(8,128)(2,1)}) fusion(bf16[128,512]{1,0:T(8,128)(2,1)} %param.20, bf16[128,512]{1,0:T(8,128)(2,1)} %param.23, bf16[128,2048]{1,0:T(8,128)(2,1)S(1)} %all_gather.10, bf16[2048,512]{1,0:T(8,128)(2,1)} %param.25), kind=kOutput, calls=%fused_computation.44 | convolution fusion | flops 268959744 | bytes 3276800 | tf_op jit(solution)/shard_map/dot_general | solution.py:115
  148.0 0.0 all-gather.5.cloned.1.call-update
  148.0 0.0 copy-start.2
  148.0 6.1 %fusion.12 = bf16[1,768,2048]{2,1,0:T(8,128)(2,1)} fusion(bf16[1,512,2048]{2,1,0:T(8,128)(2,1)} %all-gather.3.cloned.1.call-done, f32[512,768]{1,0:T(8,128)} %fusion.6, f32[512,768]{1,0:T(8,128)} %fusion.2), kind=kOutput, calls=%fused_computation.16 | convolution fusion | flops 1616117760 | bytes 8388608 | tf_op jit(solution)/shard_map/dot_general | solution.py:22
  154.2 0.6 fusion.43
  154.8 3.4 %collective-permute-start = (bf16[1,512]{1,0:T(2,128)(2,1)}, bf16[1,512]{1,0:T(2,128)(2,1)S(1)}, u32[]{:S(2)}, u32[]{:S(2)}) collective-permute-start(bf16[1,512]{1,0:T(2,128)(2,1)} %get-tuple-element.63), channel_id=1, source_target_pairs={{0,4},{4,8},{8,12},{12,16},{16,20},{20,24},{24,28},{1,5},{5,9},{9,... | collective-permute-start | bytes 3080 | tf_op jit(solution)/shard_map/ppermute | solution.py:15
  158.1 1.3 collective-permute-start.1
  159.4 0.8 copy.76
  160.3 5.8 %all-to-all-start.2 = ((bf16[128,8,256]{2,0,1:T(8,128)(2,1)}), bf16[128,8,256]{2,0,1:T(8,128)(2,1)}, u32[]{:S(2)}, u32[]{:S(2)}) async-start(bf16[128,8,256]{2,0,1:T(8,128)(2,1)} %bitcast.86), calls=%async_computation.3 | async-start | bytes 1048576 | tf_op jit(solution)/shard_map/all_to_all | solution.py:127
  166.0 5.3 %fusion.11 = bf16[1,2048,768]{1,2,0:T(8,128)(2,1)} fusion(bf16[512,768]{1,0:T(8,128)(2,1)} %copy-done.12, bf16[1,512,2048]{2,1,0:T(8,128)(2,1)} %param.16), kind=kOutput, calls=%fused_computation.15 | convolution fusion | flops 1613758464 | bytes 6029312 | tf_op jit(solution)/shard_map/dot_general | solution.py:22
  171.3 4.6 %copy.66 = bf16[1,2048,768]{2,1,0:T(8,128)(2,1)} copy(bf16[1,2048,768]{1,2,0:T(8,128)(2,1)} %fusion.10) | data formatting | bytes 6291456
  176.0 4.7 %copy.67 = bf16[1,2048,768]{2,1,0:T(8,128)(2,1)} copy(bf16[1,2048,768]{1,2,0:T(8,128)(2,1)} %fusion.11) | data formatting | bytes 6291456
  180.6 0.0 collective-permute-done
  180.6 0.7 maximum_convert_fusion
  181.4 0.8 multiply_convert_fusion.9
  182.1 0.7 multiply_convert_fusion.10
  182.8 5.7 %all-to-all-done.2 = bf16[128,8,256]{2,0,1:T(8,128)(2,1)} async-done(((bf16[128,8,256]{2,0,1:T(8,128)(2,1)}), bf16[128,8,256]{2,0,1:T(8,128)(2,1)}, u32[]{:S(2)}, u32[]{:S(2)}) %all-to-all-start.2) | async-done | bytes 524320 | tf_op jit(solution)/shard_map/all_to_all | solution.py:127
  188.5 0.8 all-gather.5.cloned.1.call-done
  189.3 2.6 %convolution_multiply_fusion = f32[256,512]{1,0:T(8,128)} fusion(bf16[1024,256]{1,0:T(8,128)(2,1)} %bitcast.14, bf16[1024,512]{1,0:T(8,128)(2,1)} %all-gather.5.cloned.1.call-done), kind=kOutput, calls=%fused_computation.30 | convolution fusion | flops 268566528 | bytes 2097152 | tf_op jit(solution)/shard_map/dot_general | solution.py:22
  (26 shorter events, 0.1 us)
Async XLA Ops:
  7.2 30.4 %copy-start = (bf16[1,2048,768]{2,1,0:T(8,128)(2,1)S(1)}, bf16[1,2048,768]{2,1,0:T(8,128)(2,1)}, u32[]{:S(2)}) copy-start(bf16[1,2048,768]{2,1,0:T(8,128)(2,1)} %param.17) | copy-start | bytes 9437188
  7.2 52.1 %all-gather.3.cloned.1.call-start = ((), (), s32[]{:S(2)}) async-start(), calls=%async_computation.4 | async-start | bytes 2621440 | tf_op jit(solution)/shard_map/all_gather | solution.py:55
  37.6 64.3 %reduce-scatter.2.cloned.1.call-start = ((), (), s32[]{:S(2)}) async-start(), calls=%async_computation.5 | async-start | bytes 2621440 | tf_op jit(solution)/shard_map/reduce_scatter | solution.py:63
  37.6 4.7 %copy-start.9 = (bf16[1,2048,768]{2,1,0:T(8,128)(2,1)S(1)}, bf16[1,2048,768]{2,1,0:T(8,128)(2,1)}, u32[]{:S(2)}) copy-start(bf16[1,2048,768]{2,1,0:T(8,128)(2,1)} %param.18) | copy-start | bytes 9437188
  37.6 4.7 %copy-start.11 = (bf16[1,512,2048]{2,1,0:T(8,128)(2,1)S(1)}, bf16[1,512,2048]{2,1,0:T(8,128)(2,1)}, u32[]{:S(2)}) copy-start(bf16[1,512,2048]{2,1,0:T(8,128)(2,1)} %param.16) | copy-start | bytes 6291460
  64.9 1.9 copy-start.13
  64.9 1.9 copy-start.12
  64.9 2.5 %copy-start.10 = (bf16[1,2048,768]{2,1,0:T(8,128)(2,1)S(1)}, bf16[1,2048,768]{2,1,0:T(8,128)(2,1)}, u32[]{:S(2)}) copy-start(bf16[1,2048,768]{2,1,0:T(8,128)(2,1)} %param.18) | copy-start | bytes 9437188
  104.7 14.0 %copy-start.8 = (s32[128,2]{0,1:T(2,128)S(1)}, s32[128,2]{0,1:T(2,128)}, u32[]{:S(2)}) copy-start(s32[128,2]{0,1:T(2,128)} %param.14) | copy-start | bytes 3076
  104.7 14.1 %copy-start.7 = (bf16[3,512]{1,0:T(4,128)(2,1)S(1)}, bf16[3,512]{1,0:T(4,128)(2,1)}, u32[]{:S(2)}) copy-start(bf16[3,512]{1,0:T(4,128)(2,1)} %param.24) | copy-start | bytes 9220
  113.0 19.9 %all-to-all-start.1 = ((bf16[8,2,16384]{2,1,0:T(2,128)(2,1)}), bf16[8,2,16384]{2,1,0:T(2,128)(2,1)}, u32[]{:S(2)}, u32[]{:S(2)}) async-start(bf16[8,2,16384]{2,1,0:T(2,128)(2,1)} %reshape.85), calls=%async_computation.2 | async-start | bytes 1048576 | tf_op jit(solution)/shard_map/all_to_all | solution.py:66
  118.5 70.8 %all-gather.5.cloned.1.call-start = ((), (), s32[]{:S(2)}) async-start(), calls=%async_computation.6 | async-start | bytes 1179648 | tf_op jit(solution)/shard_map/all_gather | solution.py:128
  118.8 17.6 %copy-start.3 = (bf16[128,512]{1,0:T(8,128)(2,1)S(1)}, bf16[128,512]{1,0:T(8,128)(2,1)}, u32[]{:S(2)}) copy-start(bf16[128,512]{1,0:T(8,128)(2,1)} %param.13) | copy-start | bytes 393220
  137.9 16.3 %copy-start.4 = (bf16[128,512]{1,0:T(8,128)(2,1)}, bf16[128,512]{1,0:T(8,128)(2,1)S(1)}, u32[]{:S(2)}) copy-start(bf16[128,512]{1,0:T(8,128)(2,1)S(1)} %fusion.25) | copy-start | bytes 393220
  144.4 0.8 copy-start.1
  148.0 11.4 %copy-start.2 = (bf16[128,2048]{1,0:T(8,128)(2,1)S(1)}, bf16[128,2048]{1,0:T(8,128)(2,1)}, u32[]{:S(2)}) copy-start(bf16[128,2048]{1,0:T(8,128)(2,1)} %copy-done.1) | copy-start | bytes 1572868
  154.8 25.9 %collective-permute-start = (bf16[1,512]{1,0:T(2,128)(2,1)}, bf16[1,512]{1,0:T(2,128)(2,1)S(1)}, u32[]{:S(2)}, u32[]{:S(2)}) collective-permute-start(bf16[1,512]{1,0:T(2,128)(2,1)} %get-tuple-element.63), channel_id=1, source_target_pairs={{0,4},{4,8},{8,12},{12,16},{16,20},{20,24},{24,28},{1,5},{5,9},{9,... | collective-permute-start | bytes 3080 | tf_op jit(solution)/shard_map/ppermute | solution.py:15
  158.1 22.5 %collective-permute-start.1 = (bf16[1,512]{1,0:T(2,128)(2,1)}, bf16[1,512]{1,0:T(2,128)(2,1)}, u32[]{:S(2)}, u32[]{:S(2)}) collective-permute-start(bf16[1,512]{1,0:T(2,128)(2,1)} %get-tuple-element.64), channel_id=1, source_target_pairs={{4,0},{8,4},{12,8},{16,12},{20,16},{24,20},{28,24},{5,1},{9,5},{13... | collective-permute-start | bytes 3080 | tf_op jit(solution)/shard_map/ppermute | solution.py:16
  160.3 28.2 %all-to-all-start.2 = ((bf16[128,8,256]{2,0,1:T(8,128)(2,1)}), bf16[128,8,256]{2,0,1:T(8,128)(2,1)}, u32[]{:S(2)}, u32[]{:S(2)}) async-start(bf16[128,8,256]{2,0,1:T(8,128)(2,1)} %bitcast.86), calls=%async_computation.3 | async-start | bytes 1048576 | tf_op jit(solution)/shard_map/all_to_all | solution.py:127
  176.0 5.4 %copy-start.5 = (bf16[128,512]{1,0:T(8,128)(2,1)S(1)}, bf16[128,512]{1,0:T(8,128)(2,1)}, u32[]{:S(2)}) copy-start(bf16[128,512]{1,0:T(8,128)(2,1)} %param.21) | copy-start | bytes 393220
  176.0 6.2 %copy-start.6 = (bf16[128,512]{1,0:T(8,128)(2,1)S(1)}, bf16[128,512]{1,0:T(8,128)(2,1)}, u32[]{:S(2)}) copy-start(bf16[128,512]{1,0:T(8,128)(2,1)} %param.22) | copy-start | bytes 393220
Sparse Core Ops, SparseCore 0:
  37.7 21.5 all-gather.2
  70.7 31.1 reduce-scatter.1
  148.1 41.1 all-gather.4
where the time goes:
time: 200 us; the launch traced here: 198 us
  waiting for transfers between devices  60.4 us (30%)
  matrix products  43.4 us (22%)
  blocking collectives  28.2 us (14%)
  local copies, waits for them, and re-layouts  27.8 us (14%)
  starting transfers between devices  16.2 us (8%)
  between operations  14 us (7%)
  other arithmetic  8.51 us (4%)
    reduce_scatter x1, waiting for transfers between devices, expert_pass(): lax.psum_scatter(jnp.stack(partials).astype(jnp.bfloat16), 'tp', scatter_...  31.1 us
    all_to_all x1, blocking collectives, expert_pass(): lax.all_to_all(outgoing, 'sp', split_axis=0, concat_axis=1, tiled=True)  21.7 us
    dot_general x5, matrix products, contract_first(): lax.dot_general(left, right, (((0,), (0,)), ((), ())), preferred_element_...  20.9 us
    unnamed x35, local copies, waits for them, and re-layouts  18.7 us
    all_gather x1, waiting for transfers between devices, expert_pass(): routed = lax.all_gather(arrived, 'tp', axis=2, tiled=True)  14 us
    dot_general x3, matrix products, contract_last(): lax.dot_general(left, right, (((1,), (1,)), ((), ())), preferred_element_...  10.6 us
    all_to_all x1, waiting for transfers between devices, expert_pass(): lax.all_to_all(summed, 'sp', split_axis=1, concat_axis=0, tiled=True)  8.71 us
    all_gather x1, blocking collectives, per_device(): resid_full = lax.all_gather(resid_grad, 'tp', axis=1, tiled=True)  6.5 us
  transfers between devices with their start and end apart: 7, of which 5 were waited for; matrix products, arithmetic and copies ran while one was open for 19% of the time, Pallas kernels for 0%

commit v1 on v0

--- a/solution.py
+++ b/solution.py
@@ -52,7 +52,7 @@
 
 def expert_pass(outgoing, input_rows, gate_weight, up_weight, down_weight):
     arrived = lax.all_to_all(outgoing, "sp", split_axis=0, concat_axis=1, tiled=True)
-    routed = lax.all_gather(arrived, "tp", axis=2, tiled=True)
+    routed = jnp.concatenate(lax.all_gather(arrived, "tp"), axis=2)
     partial_value, grad_set = expert_backward(
         input_rows[0], routed[0], gate_weight[0], up_weight[0], down_weight[0]
     )

time: 200 us -> 204 us (1.020)
  local copies, waits for them, and re-layouts: 27.8 us -> 31.9 us
    all_gather x0 -> x1, local copies, waits for them, and re-layouts: none -> 4.13 us  [expert_pass(): routed = jnp.concatenate(lax.all_gather(arrived, 'tp'), axis=2)]
where the time goes in v1:
time: 204 us; the launch traced here: 203 us
  waiting for transfers between devices  60.6 us (30%)
  matrix products  43.4 us (21%)
  local copies, waits for them, and re-layouts  31.9 us (16%)
  blocking collectives  28.5 us (14%)
  starting transfers between devices  16 us (8%)
  between operations  14 us (7%)
  other arithmetic  8.52 us (4%)
    reduce_scatter x1, waiting for transfers between devices, expert_pass(): lax.psum_scatter(jnp.stack(partials).astype(jnp.bfloat16), 'tp', scatter_...  31.1 us
    all_to_all x1, blocking collectives, expert_pass(): lax.all_to_all(outgoing, 'sp', split_axis=0, concat_axis=1, tiled=True)  21.7 us
    dot_general x5, matrix products, contract_first(): lax.dot_general(left, right, (((0,), (0,)), ((), ())), preferred_element_...  20.9 us
    unnamed x35, local copies, waits for them, and re-layouts  18.7 us
    all_gather x1, waiting for transfers between devices, expert_pass(): routed = jnp.concatenate(lax.all_gather(arrived, 'tp'), axis=2)  14 us
    dot_general x3, matrix products, contract_last(): lax.dot_general(left, right, (((1,), (1,)), ((), ())), preferred_element_...  10.6 us
    all_to_all x1, waiting for transfers between devices, expert_pass(): lax.all_to_all(summed, 'sp', split_axis=1, concat_axis=0, tiled=True)  8.89 us
    all_gather x1, blocking collectives, per_device(): resid_full = lax.all_gather(resid_grad, 'tp', axis=1, tiled=True)  6.72 us
  transfers between devices with their start and end apart: 7, of which 5 were waited for; matrix products, arithmetic and copies ran while one was open for 19% of the time, Pallas kernels for 0%

profile of v1, /device:TPU:0, one launch (start us, length us, event | category | flops | bytes accessed | tf_op | source)
XLA Modules:
  0.0 202.9 jit_solution(4610586287071647087)
XLA Ops:
  7.2 0.0 copy-start
  7.2 0.0 all-gather.3.cloned.1.call-start
  7.2 0.9 copy.73
  8.2 0.1 eq.50
  8.3 0.1 eq.46
  8.5 0.6 reduce-window.6
  9.0 0.2 slice_reduce_fusion
  9.3 0.1 fusion.37
  9.4 1.8 mul.130
  11.2 2.2 %mul.131 = f32[256,512]{1,0:T(8,128)} reshape(f32[128,2,512]{2,1,0:T(2,128)} %mul.130) | data formatting | bytes 1048576 | tf_op jit(solution)/shard_map/mul | solution.py:100
  13.4 0.8 copy.76
  14.2 0.1 mul.128
  14.4 1.4 convolution_convert_fusion
  15.8 21.7 %all_to_all.37 = bf16[8,64,512]{2,1,0:T(8,128)(2,1)} all-to-all(bf16[8,64,512]{2,1,0:T(8,128)(2,1)S(1)} %bitcast.88), channel_id=1, replica_groups=mesh['sp'=8,'tp'=4] {'sp'}, dimensions={0} | all-to-all | bytes 1048576 | tf_op jit(solution)/shard_map/all_to_all | solution.py:54
  37.5 0.0 all-gather.3.cloned.1.call-update
  37.6 0.0 reduce-scatter.2.cloned.1.call-start
  37.6 0.0 copy-start.9
  37.6 0.0 copy-start.11
  37.6 4.7 %fusion.2 = f32[512,768]{1,0:T(8,128)} fusion(bf16[1,2048,768]{2,1,0:T(8,128)(2,1)S(1)} %copy-done, bf16[1,512,2048]{2,1,0:T(8,128)(2,1)} %param.16), kind=kOutput, calls=%fused_computation.6 | convolution fusion | flops 1610612736 | bytes 6815744 | tf_op jit(solution)/shard_map/dot_general | solution.py:34
  42.3 2.9 %fusion.6 = f32[512,768]{1,0:T(8,128)} fusion(bf16[1,2048,768]{2,1,0:T(8,128)(2,1)S(1)} %copy-done.9, bf16[1,512,2048]{2,1,0:T(8,128)(2,1)S(1)} %copy-done.11), kind=kOutput, calls=%fused_computation.10 | convolution fusion | flops 1610612736 | bytes 6815744 | tf_op jit(solution)/shard_map/dot_general | solution.py:35
  45.3 14.0 %all-gather.3.cloned.1.call-done = bf16[4,1,512,512]{3,2,1,0:T(8,128)(2,1)} async-done(((bf16[1,1,512,512]{3,2,1,0:T(8,128)(2,1)}), bf16[4,1,512,512]{3,2,1,0:T(8,128)(2,1)}) %all-gather.3.cloned.1.call-update) | async-done | bytes 2097168 | tf_op jit(solution)/shard_map/all_gather | solution.py:55
  59.3 4.1 %copy.77 = bf16[4,1,512,512]{2,3,0,1:T(8,128)(2,1)} copy(bf16[4,1,512,512]{3,2,1,0:T(8,128)(2,1)} %all-gather.3.cloned.1.call-done) | data formatting | bytes 4194304 | tf_op jit(solution)/shard_map/all_gather | solution.py:55
  63.4 5.6 %multiply_convert_fusion.4 = (bf16[512,768]{1,0:T(8,128)(2,1)S(1)}, bf16[512,768]{1,0:T(8,128)(2,1)S(1)}) fusion(f32[512,768]{1,0:T(8,128)} %fusion.2, f32[512,768]{1,0:T(8,128)} %fusion.6, bf16[512,2048]{0,1:T(8,128)(2,1)} %bitcast.84, bf16[1,768,2048]{2,1,0:T(8,128)(2,1)} %param.19), kind=kOutput, calls=%fused_computation.23 | convolution fusion | flops 1615724544 | bytes 9961472 | tf_op jit(solution)/shard_map/dot_general | solution.py:28
  69.1 0.0 copy-start.10
  69.1 1.8 fusion
  70.9 0.6 copy-done.10
  71.5 3.1 %fusion.15 = bf16[1,512,2048]{2,1,0:T(8,128)(2,1)} fusion(f32[512,2048]{1,0:T(8,128)S(1)} %fusion, bf16[512,768]{1,0:T(8,128)(2,1)S(1)} %get-tuple-element.66, bf16[1,2048,768]{2,1,0:T(8,128)(2,1)S(1)} %copy-done.10), kind=kOutput, calls=%fused_computation.17 | convolution fusion | flops 1612709888 | bytes 10223616 | tf_op jit(solution)/shard_map/dot_general | solution.py:28
  74.7 0.0 reduce-scatter.2.cloned.1.call-update
  74.7 0.1 reduce_sum.24
  74.8 0.1 copy.75
  74.9 31.1 %reduce-scatter.2.cloned.1.call-done = bf16[1,512,512]{2,1,0:T(8,128)(2,1)} async-done(((bf16[1,512,2048]{2,1,0:T(8,128)(2,1)}), bf16[1,512,512]{2,1,0:T(8,128)(2,1)}) %reduce-scatter.2.cloned.1.call-update) | async-done | bytes 524304 | tf_op jit(solution)/shard_map/reduce_scatter | solution.py:63
  106.0 2.8 %copy.91 = bf16[1,512,512]{2,0,1:T(2,128)(2,1)} copy(bf16[1,512,512]{2,1,0:T(8,128)(2,1)} %reduce-scatter.2.cloned.1.call-done) | data formatting | bytes 1048576 | tf_op jit(solution)/shard_map/reduce_scatter | solution.py:63
  108.9 0.5 broadcast.62
  109.4 5.6 %reduce.3 = bf16[512,512]{1,0:T(8,128)(2,1)} reduce(bf16[512,1,512]{2,1,0:T(2,128)(2,1)} %bitcast.82, bf16[]{:T(256)} %broadcast.62), dimensions={1}, to_apply=%bitcast.80.reduce_sub_computation | reduce | bytes 1048578
  114.9 2.2 %reshape.90 = bf16[8,2,16384]{2,1,0:T(2,128)(2,1)} reshape(bf16[512,512]{1,0:T(8,128)(2,1)} %reduce.3) | data formatting | bytes 1048576
  117.1 5.5 %all-to-all-start.1 = ((bf16[8,2,16384]{2,1,0:T(2,128)(2,1)}), bf16[8,2,16384]{2,1,0:T(2,128)(2,1)}, u32[]{:S(2)}, u32[]{:S(2)}) async-start(bf16[8,2,16384]{2,1,0:T(2,128)(2,1)} %reshape.90), calls=%async_computation.2 | async-start | bytes 1048576 | tf_op jit(solution)/shard_map/all_to_all | solution.py:66
  122.7 0.0 all-gather.5.cloned.1.call-start
  122.7 0.1 fusion.31
  122.8 0.0 copy-start.3
  122.8 5.4 %fusion.10 = bf16[1,2048,768]{1,2,0:T(8,128)(2,1)} fusion(bf16[512,768]{1,0:T(8,128)(2,1)} %copy-done.13, bf16[1,512,2048]{2,1,0:T(8,128)(2,1)} %param.16), kind=kOutput, calls=%fused_computation.14 | convolution fusion | flops 1613758464 | bytes 6029312 | tf_op jit(solution)/shard_map/dot_general | solution.py:22
  128.2 8.9 %all-to-all-done.1 = bf16[8,2,16384]{2,1,0:T(2,128)(2,1)} async-done(((bf16[8,2,16384]{2,1,0:T(2,128)(2,1)}), bf16[8,2,16384]{2,1,0:T(2,128)(2,1)}, u32[]{:S(2)}, u32[]{:S(2)}) %all-to-all-start.1) | async-done | bytes 524320 | tf_op jit(solution)/shard_map/all_to_all | solution.py:66
  137.1 3.5 %reshape.91 = bf16[512,1,512]{2,1,0:T(2,128)(2,1)} reshape(bf16[8,2,16384]{2,1,0:T(2,128)(2,1)} %all-to-all-done.1) | data formatting | bytes 1048576
  140.6 1.5 fusion.23
  142.1 0.0 copy-start.4
  142.1 6.7 %all_gather.14 = bf16[128,2048]{1,0:T(8,128)(2,1)S(1)} all-gather(bf16[128,512]{1,0:T(8,128)(2,1)S(1)} %fusion.23), channel_id=1, replica_groups=mesh['sp'=8,'tp'=4] {'tp'}, dimensions={1}, use_global_device_ids=true | all-gather | bytes 655360 | tf_op jit(solution)/shard_map/all_gather | solution.py:114
  148.8 0.8 copy-done.1
  149.6 2.8 %fusion.29 = (bf16[128,512]{1,0:T(8,128)(2,1)S(1)}, bf16[128,512]{1,0:T(8,128)(2,1)}, bf16[128,512]{1,0:T(8,128)(2,1)}) fusion(bf16[128,512]{1,0:T(8,128)(2,1)} %param.20, bf16[128,512]{1,0:T(8,128)(2,1)} %param.23, bf16[128,2048]{1,0:T(8,128)(2,1)S(1)} %all_gather.14, bf16[2048,512]{1,0:T(8,128)(2,1)} %param.25), kind=kOutput, calls=%fused_computation.42 | convolution fusion | flops 268959744 | bytes 3276800 | tf_op jit(solution)/shard_map/dot_general | solution.py:115
  152.4 0.0 all-gather.5.cloned.1.call-update
  152.4 0.0 copy-start.2
  152.4 6.1 %fusion.12 = bf16[1,768,2048]{2,1,0:T(8,128)(2,1)} fusion(bf16[512,2048]{0,1:T(8,128)(2,1)} %bitcast.85, f32[512,768]{1,0:T(8,128)} %fusion.6, f32[512,768]{1,0:T(8,128)} %fusion.2), kind=kOutput, calls=%fused_computation.16 | convolution fusion | flops 1616117760 | bytes 8388608 | tf_op jit(solution)/shard_map/dot_general | solution.py:22
  158.6 0.6 fusion.41
  159.1 3.4 %collective-permute-start = (bf16[1,512]{1,0:T(2,128)(2,1)}, bf16[1,512]{1,0:T(2,128)(2,1)S(1)}, u32[]{:S(2)}, u32[]{:S(2)}) collective-permute-start(bf16[1,512]{1,0:T(2,128)(2,1)} %get-tuple-element.71), channel_id=1, source_target_pairs={{0,4},{4,8},{8,12},{12,16},{16,20},{20,24},{24,28},{1,5},{5,9},{9,... | collective-permute-start | bytes 3080 | tf_op jit(solution)/shard_map/ppermute | solution.py:15
  162.5 1.3 collective-permute-start.1
  163.8 0.8 copy.90
  164.6 5.8 %all-to-all-start.2 = ((bf16[128,8,256]{2,0,1:T(8,128)(2,1)}), bf16[128,8,256]{2,0,1:T(8,128)(2,1)}, u32[]{:S(2)}, u32[]{:S(2)}) async-start(bf16[128,8,256]{2,0,1:T(8,128)(2,1)} %bitcast.86), calls=%async_computation.3 | async-start | bytes 1048576 | tf_op jit(solution)/shard_map/all_to_all | solution.py:127
  170.4 5.3 %fusion.11 = bf16[1,2048,768]{1,2,0:T(8,128)(2,1)} fusion(bf16[512,768]{1,0:T(8,128)(2,1)} %copy-done.12, bf16[1,512,2048]{2,1,0:T(8,128)(2,1)} %param.16), kind=kOutput, calls=%fused_computation.15 | convolution fusion | flops 1613758464 | bytes 6029312 | tf_op jit(solution)/shard_map/dot_general | solution.py:22
  175.7 4.6 %copy.80 = bf16[1,2048,768]{2,1,0:T(8,128)(2,1)} copy(bf16[1,2048,768]{1,2,0:T(8,128)(2,1)} %fusion.10) | data formatting | bytes 6291456
  180.4 4.7 %copy.81 = bf16[1,2048,768]{2,1,0:T(8,128)(2,1)} copy(bf16[1,2048,768]{1,2,0:T(8,128)(2,1)} %fusion.11) | data formatting | bytes 6291456
  185.0 0.7 maximum_convert_fusion
  185.8 0.8 multiply_convert_fusion.9
  186.5 0.7 multiply_convert_fusion.10
  187.2 5.7 %all-to-all-done.2 = bf16[128,8,256]{2,0,1:T(8,128)(2,1)} async-done(((bf16[128,8,256]{2,0,1:T(8,128)(2,1)}), bf16[128,8,256]{2,0,1:T(8,128)(2,1)}, u32[]{:S(2)}, u32[]{:S(2)}) %all-to-all-start.2) | async-done | bytes 524320 | tf_op jit(solution)/shard_map/all_to_all | solution.py:127
  192.9 0.8 all-gather.5.cloned.1.call-done
  193.7 2.6 %convolution_multiply_fusion = f32[256,512]{1,0:T(8,128)} fusion(bf16[1024,256]{1,0:T(8,128)(2,1)} %bitcast.15, bf16[1024,512]{1,0:T(8,128)(2,1)} %all-gather.5.cloned.1.call-done), kind=kOutput, calls=%fused_computation.28 | convolution fusion | flops 268566528 | bytes 2097152 | tf_op jit(solution)/shard_map/dot_general | solution.py:22
  (27 shorter events, 0.1 us)
Async XLA Ops:
  7.2 30.4 %copy-start = (bf16[1,2048,768]{2,1,0:T(8,128)(2,1)S(1)}, bf16[1,2048,768]{2,1,0:T(8,128)(2,1)}, u32[]{:S(2)}) copy-start(bf16[1,2048,768]{2,1,0:T(8,128)(2,1)} %param.17) | copy-start | bytes 9437188
  7.2 52.1 %all-gather.3.cloned.1.call-start = ((), (), s32[]{:S(2)}) async-start(), calls=%async_computation.4 | async-start | bytes 2621440 | tf_op jit(solution)/shard_map/all_gather | solution.py:55
  37.6 68.5 %reduce-scatter.2.cloned.1.call-start = ((), (), s32[]{:S(2)}) async-start(), calls=%async_computation.5 | async-start | bytes 2621440 | tf_op jit(solution)/shard_map/reduce_scatter | solution.py:63
  37.6 4.7 %copy-start.9 = (bf16[1,2048,768]{2,1,0:T(8,128)(2,1)S(1)}, bf16[1,2048,768]{2,1,0:T(8,128)(2,1)}, u32[]{:S(2)}) copy-start(bf16[1,2048,768]{2,1,0:T(8,128)(2,1)} %param.18) | copy-start | bytes 9437188
  37.6 4.7 %copy-start.11 = (bf16[1,512,2048]{2,1,0:T(8,128)(2,1)S(1)}, bf16[1,512,2048]{2,1,0:T(8,128)(2,1)}, u32[]{:S(2)}) copy-start(bf16[1,512,2048]{2,1,0:T(8,128)(2,1)} %param.16) | copy-start | bytes 6291460
  69.0 1.9 copy-start.13
  69.1 1.9 copy-start.12
  69.1 2.5 %copy-start.10 = (bf16[1,2048,768]{2,1,0:T(8,128)(2,1)S(1)}, bf16[1,2048,768]{2,1,0:T(8,128)(2,1)}, u32[]{:S(2)}) copy-start(bf16[1,2048,768]{2,1,0:T(8,128)(2,1)} %param.18) | copy-start | bytes 9437188
  108.9 13.9 %copy-start.8 = (s32[128,2]{0,1:T(2,128)S(1)}, s32[128,2]{0,1:T(2,128)}, u32[]{:S(2)}) copy-start(s32[128,2]{0,1:T(2,128)} %param.14) | copy-start | bytes 3076
  108.9 13.9 %copy-start.7 = (bf16[3,512]{1,0:T(4,128)(2,1)S(1)}, bf16[3,512]{1,0:T(4,128)(2,1)}, u32[]{:S(2)}) copy-start(bf16[3,512]{1,0:T(4,128)(2,1)} %param.24) | copy-start | bytes 9220
  117.1 19.9 %all-to-all-start.1 = ((bf16[8,2,16384]{2,1,0:T(2,128)(2,1)}), bf16[8,2,16384]{2,1,0:T(2,128)(2,1)}, u32[]{:S(2)}, u32[]{:S(2)}) async-start(bf16[8,2,16384]{2,1,0:T(2,128)(2,1)} %reshape.90), calls=%async_computation.2 | async-start | bytes 1048576 | tf_op jit(solution)/shard_map/all_to_all | solution.py:66
  122.7 71.1 %all-gather.5.cloned.1.call-start = ((), (), s32[]{:S(2)}) async-start(), calls=%async_computation.6 | async-start | bytes 1179648 | tf_op jit(solution)/shard_map/all_gather | solution.py:128
  122.8 17.7 %copy-start.3 = (bf16[128,512]{1,0:T(8,128)(2,1)S(1)}, bf16[128,512]{1,0:T(8,128)(2,1)}, u32[]{:S(2)}) copy-start(bf16[128,512]{1,0:T(8,128)(2,1)} %param.13) | copy-start | bytes 393220
  142.1 16.5 %copy-start.4 = (bf16[128,512]{1,0:T(8,128)(2,1)}, bf16[128,512]{1,0:T(8,128)(2,1)S(1)}, u32[]{:S(2)}) copy-start(bf16[128,512]{1,0:T(8,128)(2,1)S(1)} %fusion.23) | copy-start | bytes 393220
  148.8 0.8 copy-start.1
  152.4 11.4 %copy-start.2 = (bf16[128,2048]{1,0:T(8,128)(2,1)S(1)}, bf16[128,2048]{1,0:T(8,128)(2,1)}, u32[]{:S(2)}) copy-start(bf16[128,2048]{1,0:T(8,128)(2,1)} %copy-done.1) | copy-start | bytes 1572868
  159.1 25.9 %collective-permute-start = (bf16[1,512]{1,0:T(2,128)(2,1)}, bf16[1,512]{1,0:T(2,128)(2,1)S(1)}, u32[]{:S(2)}, u32[]{:S(2)}) collective-permute-start(bf16[1,512]{1,0:T(2,128)(2,1)} %get-tuple-element.71), channel_id=1, source_target_pairs={{0,4},{4,8},{8,12},{12,16},{16,20},{20,24},{24,28},{1,5},{5,9},{9,... | collective-permute-start | bytes 3080 | tf_op jit(solution)/shard_map/ppermute | solution.py:15
  162.5 22.5 %collective-permute-start.1 = (bf16[1,512]{1,0:T(2,128)(2,1)}, bf16[1,512]{1,0:T(2,128)(2,1)}, u32[]{:S(2)}, u32[]{:S(2)}) collective-permute-start(bf16[1,512]{1,0:T(2,128)(2,1)} %get-tuple-element.72), channel_id=1, source_target_pairs={{4,0},{8,4},{12,8},{16,12},{20,16},{24,20},{28,24},{5,1},{9,5},{13... | collective-permute-start | bytes 3080 | tf_op jit(solution)/shard_map/ppermute | solution.py:16
  164.6 28.2 %all-to-all-start.2 = ((bf16[128,8,256]{2,0,1:T(8,128)(2,1)}), bf16[128,8,256]{2,0,1:T(8,128)(2,1)}, u32[]{:S(2)}, u32[]{:S(2)}) async-start(bf16[128,8,256]{2,0,1:T(8,128)(2,1)} %bitcast.86), calls=%async_computation.3 | async-start | bytes 1048576 | tf_op jit(solution)/shard_map/all_to_all | solution.py:127
  180.4 5.4 %copy-start.5 = (bf16[128,512]{1,0:T(8,128)(2,1)S(1)}, bf16[128,512]{1,0:T(8,128)(2,1)}, u32[]{:S(2)}) copy-start(bf16[128,512]{1,0:T(8,128)(2,1)} %param.21) | copy-start | bytes 393220
  180.4 6.2 %copy-start.6 = (bf16[128,512]{1,0:T(8,128)(2,1)S(1)}, bf16[128,512]{1,0:T(8,128)(2,1)}, u32[]{:S(2)}) copy-start(bf16[128,512]{1,0:T(8,128)(2,1)} %param.22) | copy-start | bytes 393220
Sparse Core Ops, SparseCore 0:
  37.7 21.5 all-gather.2
  74.8 31.1 reduce-scatter.1
  152.5 41.1 all-gather.4
